TPU v7x, 32 devices: a whole 2x2x4 slice. The times are simulated.
32 devices in a mesh: sp: 8 (over z, x), tp: 4 (over y, core).
Axes of the slice: x: 2, y: 2, z: 4, core: 2. Of those that a mesh axis runs over, the one named last changes fastest.
Arguments:
- queries: bfloat16 [1024, 2048], P('sp', 'tp'), may hold values from -440 to 440
- key_rows: bfloat16 [1024, 1024], P('sp', 'tp'), may hold values from -6 to 6
- value_rows: bfloat16 [1024, 1024], P('sp', 'tp'), may hold values from -6 to 6
- sink_logits: float32 [32], P('tp'), may hold values from -6 to 6
- out_weight: bfloat16 [2048, 2048], P('tp'), may hold values from -0.125 to 0.125
- residual: bfloat16 [1024, 2048], P('sp'), may hold values from -3 to 3
- norm_gain: float32 [2048], replicated, may hold values from 0.1 to 1.9
- routes: int32 [1024, 2], P('sp'), may hold values from 0 to 7, all different within a row; in each aligned block of 128 rows (0 to 127, 128 to 255, ...) at most 64 rows name the same one
- route_weights: float32 [1024, 2], P('sp'), may hold values from 0.2 to 1
- gate_weight: bfloat16 [8, 2048, 4096], P('sp', None, 'tp'), may hold values from -0.125 to 0.125
- up_weight: bfloat16 [8, 2048, 4096], P('sp', None, 'tp'), may hold values from -0.125 to 0.125
- down_weight: bfloat16 [8, 4096, 2048], P('sp', 'tp'), may hold values from -0.09375 to 0.09375
Outputs:
- layer_out: bfloat16 [1024, 2048], P('sp')
Inputs may be any that keep to these rules, and one draw needn't show every extreme that they name: `routes`: each row names 2 different experts. In each aligned block of 128 rows (the rows of one index of sp) no expert is named by more than 64 rows, a bound that some block reaches.
All inputs are finite; a program needn't handle non-finite values.
Results may differ from a plain program's by a relative error of at most 0.02.
Values may be sent and summed in bfloat16 or wider, within the bound.
A program may use at most 64 MiB of HBM per device.

v0:
```python
import jax
import jax.numpy as jnp
from jax import lax
from jax.sharding import PartitionSpec as P

HEAD_DIM = 64
QH = 32
WINDOW = 128
TOP = 2


def from_behind(array, axis, by):
    peers = lax.axis_size(axis)
    pairs = [(i, i + by) for i in range(peers) if 0 <= i + by < peers]
    return lax.ppermute(array, axis, pairs)


def per_device(
    queries,
    key_rows,
    value_rows,
    sink_logits,
    out_weight,
    residual,
    norm_gain,
    routes,
    route_weights,
    gate_weight,
    up_weight,
    down_weight,
):
    rows_here = queries.shape[0]
    width = residual.shape[1]
    heads_here = queries.shape[1] // HEAD_DIM
    kv_here = key_rows.shape[1] // HEAD_DIM
    group_size = heads_here // kv_here
    blocks = rows_here // WINDOW
    rim_rows = jnp.stack([key_rows, value_rows])
    before = from_behind(rim_rows, "sp", 1)
    key_ext = jnp.concatenate([before[0], key_rows], axis=0).reshape(
        blocks + 1, WINDOW, kv_here, HEAD_DIM
    )
    val_ext = jnp.concatenate([before[1], value_rows], axis=0).reshape(
        blocks + 1, WINDOW, kv_here, HEAD_DIM
    )
    key_pair = jnp.concatenate([key_ext[:-1], key_ext[1:]], axis=1)
    val_pair = jnp.concatenate([val_ext[:-1], val_ext[1:]], axis=1)
    query_blocks = queries.reshape(blocks, WINDOW, kv_here, group_size, HEAD_DIM)
    scores = jnp.einsum(
        "bqkgd,bckd->bkgqc", query_blocks, key_pair, preferred_element_type=jnp.float32
    ) * HEAD_DIM ** (-0.5)
    distance = jnp.arange(WINDOW)[:, None] + WINDOW - jnp.arange(2 * WINDOW)[None, :]
    offset = lax.axis_index("sp") * rows_here
    key_global = (
        offset
        + jnp.arange(blocks)[:, None, None] * WINDOW
        + jnp.arange(2 * WINDOW)[None, None, :]
        - WINDOW
    )
    allowed = (distance >= 0)[None] & (distance <= WINDOW)[None] & (key_global >= 0)
    head_ids = lax.axis_index("tp") * heads_here + jnp.arange(heads_here)
    slopes = jnp.exp2(-8.0 * (head_ids + 1).astype(jnp.float32) / QH).reshape(kv_here, group_size)
    scores = scores - slopes[None, :, :, None, None] * distance.astype(jnp.float32)
    scores = jnp.where(allowed[:, None, None], scores, -jnp.inf)
    row_peak = jnp.max(scores, axis=-1, keepdims=True)
    log_total = row_peak + jnp.log(jnp.sum(jnp.exp(scores - row_peak), axis=-1, keepdims=True))
    weights_bf = jnp.exp(scores - log_total).astype(jnp.bfloat16)
    attended = jnp.einsum(
        "bkgqc,bckd->bqkgd", weights_bf, val_pair, preferred_element_type=jnp.float32
    )
    keep_factor = jax.nn.sigmoid(
        log_total[..., 0] - sink_logits.reshape(kv_here, group_size)[None, :, :, None]
    )
    keep_factor = jnp.transpose(keep_factor, (0, 3, 1, 2))[..., None]
    attended = (
        (attended * keep_factor).astype(jnp.bfloat16).reshape(rows_here, heads_here * HEAD_DIM)
    )
    partial_value = jnp.dot(attended, out_weight, preferred_element_type=jnp.float32)
    partial_value = lax.optimization_barrier(partial_value.astype(jnp.bfloat16)).astype(jnp.float32)
    head_total = lax.psum(partial_value.astype(jnp.bfloat16), "tp").astype(jnp.float32)
    mixed_state = (residual.astype(jnp.float32) + head_total).astype(jnp.bfloat16)
    state32 = mixed_state.astype(jnp.float32)
    normed = (
        state32 * lax.rsqrt(jnp.mean(state32 * state32, axis=-1, keepdims=True) + 1e-06) * norm_gain
    ).astype(jnp.bfloat16)
    experts = lax.axis_size("sp")
    capacity = 2 * rows_here * TOP // experts
    flat_routes = routes.reshape(-1)
    member = (flat_routes[:, None] == jnp.arange(experts)[None, :]).astype(jnp.int32)
    slot_rank = jnp.sum((jnp.cumsum(member, axis=0) - 1) * member, axis=1)
    slot_index = flat_routes * capacity + slot_rank
    picker = (jnp.arange(experts * capacity)[:, None] == slot_index[None, :]).astype(jnp.int32)
    picker = jnp.sum(picker.reshape(experts * capacity, rows_here, TOP), axis=-1).astype(
        jnp.bfloat16
    )
    outgoing = (
        jnp.dot(picker, normed, preferred_element_type=jnp.float32)
        .astype(jnp.bfloat16)
        .reshape(experts, capacity, width)
    )
    w_gate = gate_weight[0]
    w_up = up_weight[0]
    w_down = down_weight[0]
    slot_share = capacity // lax.axis_size("tp")
    mine = lax.dynamic_slice_in_dim(outgoing, lax.axis_index("tp") * slot_share, slot_share, 1)
    arrived = lax.all_to_all(mine, "sp", split_axis=0, concat_axis=0, tiled=True)
    gathered = lax.all_gather(arrived, "tp", axis=1, tiled=True)
    flat_rows = gathered.reshape(-1, width)
    gate_pre = jnp.dot(flat_rows, w_gate, preferred_element_type=jnp.float32)
    up_pre = jnp.dot(flat_rows, w_up, preferred_element_type=jnp.float32)
    activated = (jax.nn.silu(gate_pre) * up_pre).astype(jnp.bfloat16)
    result = jnp.dot(activated, w_down, preferred_element_type=jnp.float32)
    result = lax.optimization_barrier(result.astype(jnp.bfloat16)).astype(jnp.float32)
    summed = lax.psum_scatter(
        result.reshape(gathered.shape).astype(jnp.bfloat16), "tp", scatter_dimension=1, tiled=True
    )
    back_rows = lax.all_to_all(summed, "sp", split_axis=0, concat_axis=0, tiled=True)
    returned = lax.all_gather(back_rows, "tp", axis=1, tiled=True)
    slot_table = returned.reshape(experts * capacity, width)
    picked = jnp.take(slot_table, slot_index, axis=0).reshape(rows_here, TOP, width)
    expert_mix = jnp.sum(route_weights[..., None] * picked.astype(jnp.float32), axis=1)
    return (state32 + expert_mix).astype(jnp.bfloat16)


def solution(mesh):
    placed = (
        P("sp", "tp"),
        P("sp", "tp"),
        P("sp", "tp"),
        P("tp"),
        P("tp", None),
        P("sp", None),
        P(),
        P("sp", None),
        P("sp", None),
        P("sp", None, "tp"),
        P("sp", None, "tp"),
        P("sp", "tp", None),
    )
    return jax.shard_map(
        per_device, mesh=mesh, in_specs=placed, out_specs=P("sp", None), check_vma=False
    )
```

profile of v0, /device:TPU:3, one launch (start us, length us, event | category | flops | bytes accessed | tf_op | source)
XLA Modules:
  0.0 207.4 jit_solution(12147156466361507940)
XLA Ops:
  6.5 1.0 pad_maximum_fusion
  7.6 3.2 %collective-permute-start = (bf16[2,128,256]{2,1,0:T(8,128)(2,1)S(1)}, bf16[2,128,256]{2,1,0:T(8,128)(2,1)S(1)}, u32[]{:S(2)}, u32[]{:S(2)}) collective-permute-start(bf16[2,128,256]{2,1,0:T(8,128)(2,1)S(1)} %pad_maximum_fusion), channel_id=1, source_target_pairs={{0,4},{4,8},{8,12},{12,16},{16,20},{20,24},{24,28},{1,5},{5,9},{9,... | collective-permute-start | bytes 393224 | tf_op jit(solution)/shard_map/ppermute | solution.py:15
  10.8 0.8 copy.50
  12.0 0.6 reduce-window.6
  12.9 1.0 copy.46
  13.9 1.0 copy.44
  14.9 1.0 copy.47
  15.9 0.7 sub.85
  17.1 0.4 fusion.51
  18.2 1.3 convolution_convert_fusion.1
  19.6 33.0 %all-reduce.2.cloned.1.call-done = bf16[128,2048]{1,0:T(8,128)(2,1)} async-done(((bf16[128,2048]{1,0:T(8,128)(2,1)}), bf16[128,2048]{1,0:T(8,128)(2,1)}) %all-reduce.2.cloned.1.call-update) | async-done | bytes 524304 | tf_op jit(solution)/shard_map/psum | solution.py:80
  52.6 1.3 fusion.16
  53.9 1.8 convolution_convert_fusion
  55.8 18.6 %all_to_all.10 = bf16[8,16,2048]{2,1,0:T(8,128)(2,1)} all-to-all(bf16[8,16,2048]{2,1,0:T(8,128)(2,1)S(1)} %constant_dynamic-slice_fusion), channel_id=1, replica_groups=mesh['sp'=8,'tp'=4] {'sp'}, dimensions={0} | all-to-all | bytes 1048576 | tf_op jit(solution)/shard_map/all_to_all | solution.py:106
  74.4 23.0 %all-gather.3.cloned.1.call-done = bf16[8,64,2048]{2,1,0:T(8,128)(2,1)} async-done(((bf16[8,16,2048]{2,1,0:T(8,128)(2,1)}), bf16[8,64,2048]{2,1,0:T(8,128)(2,1)}) %all-gather.3.cloned.1.call-update) | async-done | bytes 2097168 | tf_op jit(solution)/shard_map/all_gather | solution.py:107
  97.4 6.5 %fusion.4 = f32[512,1024]{1,0:T(8,128)} fusion(bf16[512,2048]{1,0:T(8,128)(2,1)} %bitcast.102, bf16[1,2048,1024]{2,1,0:T(8,128)(2,1)} %param.21), kind=kOutput, calls=%fused_computation.5 | convolution fusion | flops 2147483648 | bytes 8388608 | tf_op jit(solution)/shard_map/dot_general | solution.py:109
  103.9 10.5 %fusion.6 = bf16[512,2048]{1,0:T(8,128)(2,1)} fusion(bf16[1,1024,2048]{2,1,0:T(8,128)(2,1)} %param.23, f32[512,1024]{1,0:T(8,128)} %fusion.4, bf16[512,2048]{1,0:T(8,128)(2,1)} %bitcast.103, bf16[1,2048,1024]{2,1,0:T(8,128)(2,1)} %param.22), kind=kOutput, calls=%fused_computation.7 | convolution fusion | flops 4299161600 | bytes 14680064 | tf_op jit(solution)/shard_map/dot_general | solution.py:112
  114.5 30.7 %reduce-scatter.2.cloned.1.call-done = bf16[8,16,2048]{2,1,0:T(8,128)(2,1)} async-done(((bf16[8,64,2048]{2,1,0:T(8,128)(2,1)}), bf16[8,16,2048]{2,1,0:T(8,128)(2,1)}) %reduce-scatter.2.cloned.1.call-update) | async-done | bytes 524304 | tf_op jit(solution)/shard_map/reduce_scatter | solution.py:114
  145.2 18.9 %all_to_all.11 = bf16[8,16,2048]{2,1,0:T(8,128)(2,1)} all-to-all(bf16[8,16,2048]{2,1,0:T(8,128)(2,1)} %reduce-scatter.2.cloned.1.call-done), channel_id=1, replica_groups=mesh['sp'=8,'tp'=4] {'sp'}, dimensions={0} | all-to-all | bytes 1048576 | tf_op jit(solution)/shard_map/all_to_all | solution.py:117
  164.7 21.9 %all-gather.5.cloned.1.call-done = bf16[8,64,2048]{2,1,0:T(8,128)(2,1)} async-done(((bf16[8,16,2048]{2,1,0:T(8,128)(2,1)}), bf16[8,64,2048]{2,1,0:T(8,128)(2,1)}) %all-gather.5.cloned.1.call-update) | async-done | bytes 2097168 | tf_op jit(solution)/shard_map/all_gather | solution.py:118
  186.6 5.2 %gather_fusion = bf16[256,2048]{1,0:T(8,128)(2,1)} fusion(bf16[512,2048]{1,0:T(8,128)(2,1)} %bitcast.89, s32[1024]{0:T(1024)S(1)} %pad_clamp_fusion), kind=kCustom, calls=%fused_computation | custom fusion | bytes 2098176 | tf_op jit(solution)/shard_map/jit(_take)/gather | solution.py:120
  191.8 2.6 %gather.7 = bf16[128,2,2048]{2,1,0:T(2,128)(2,1)} reshape(bf16[256,2048]{1,0:T(8,128)(2,1)} %gather_fusion) | data formatting | bytes 2097152 | tf_op jit(solution)/shard_map/jit(_take)/gather | solution.py:120
  194.4 5.5 %multiply_reduce_fusion = f32[128,2048]{1,0:T(8,128)S(1)} fusion(bf16[128,2,2048]{2,1,0:T(2,128)(2,1)} %gather.7, pred[128,2]{1,0:T(8,128)(4,1)S(1)} %copy.53, f32[128,2]{1,0:T(8,128)S(1)} %copy.49), kind=kLoop, calls=%fused_computation.10 | loop fusion | flops 1835008 | bytes 2098432 | tf_op jit(solution)/shard_map/reduce_sum | solution.py:121
  199.9 1.0 fusion.19
  (52 shorter events, 2.6 us)
Async XLA Ops:
  6.5 11.6 %copy-start = (bf16[512,2048]{1,0:T(8,128)(2,1)S(1)}, bf16[512,2048]{1,0:T(8,128)(2,1)}, u32[]{:S(2)}) copy-start(bf16[512,2048]{1,0:T(8,128)(2,1)} %param.16) | copy-start | bytes 6291460
  6.5 46.0 %all-reduce.2.cloned.1.call-start = ((), (), s32[]{:S(2)}) async-start(), calls=%async_computation.3 | async-start | bytes 1048576 | tf_op jit(solution)/shard_map/psum | solution.py:80
  7.6 9.3 %collective-permute-start = (bf16[2,128,256]{2,1,0:T(8,128)(2,1)S(1)}, bf16[2,128,256]{2,1,0:T(8,128)(2,1)S(1)}, u32[]{:S(2)}, u32[]{:S(2)}) collective-permute-start(bf16[2,128,256]{2,1,0:T(8,128)(2,1)S(1)} %pad_maximum_fusion), channel_id=1, source_target_pairs={{0,4},{4,8},{8,12},{12,16},{16,20},{20,24},{24,28},{1,5},{5,9},{9,... | collective-permute-start | bytes 393224 | tf_op jit(solution)/shard_map/ppermute | solution.py:15
  17.8 1.7 copy-start.3
  18.1 34.4 %copy-start.1 = (bf16[128,2048]{1,0:T(8,128)(2,1)S(1)}, bf16[128,2048]{1,0:T(8,128)(2,1)}, u32[]{:S(2)}) copy-start(bf16[128,2048]{1,0:T(8,128)(2,1)} %param.17) | copy-start | bytes 1572868
  18.1 35.7 %copy-start.4 = (f32[2048]{0:T(1024)S(1)}, f32[2048]{0:T(1024)}, u32[]{:S(2)}) copy-start(f32[2048]{0:T(1024)} %param.18) | copy-start | bytes 24580
  19.4 77.9 %all-gather.3.cloned.1.call-start = ((), (), s32[]{:S(2)}) async-start(), calls=%async_computation.4 | async-start | bytes 2621440 | tf_op jit(solution)/shard_map/all_gather | solution.py:107
  74.3 70.9 %reduce-scatter.2.cloned.1.call-start = ((), (), s32[]{:S(2)}) async-start(), calls=%async_computation.5 | async-start | bytes 2621440 | tf_op jit(solution)/shard_map/reduce_scatter | solution.py:114
  114.4 50.1 %copy-start.5 = (f32[128,2]{0,1:T(2,128)S(1)}, f32[128,2]{0,1:T(2,128)}, u32[]{:S(2)}) copy-start(f32[128,2]{0,1:T(2,128)} %param.20) | copy-start | bytes 3076
  114.4 72.1 %all-gather.5.cloned.1.call-start = ((), (), s32[]{:S(2)}) async-start(), calls=%async_computation.6 | async-start | bytes 2621440 | tf_op jit(solution)/shard_map/all_gather | solution.py:118
  191.8 8.1 %copy-start.2 = (bf16[128,2048]{1,0:T(8,128)(2,1)S(1)}, bf16[128,2048]{1,0:T(8,128)(2,1)}, u32[]{:S(2)}) copy-start(bf16[128,2048]{1,0:T(8,128)(2,1)} %all-reduce.2.cloned.1.call-done) | copy-start | bytes 1572868
Sparse Core Ops, SparseCore 0:
  19.6 32.9 all-reduce.1
  74.5 22.8 all-gather.2
  114.6 30.6 reduce-scatter.1
  164.2 22.2 all-gather.4
where the time goes:
time: 209 us; the launch traced here: 207 us
  waiting for transfers between devices  109 us (52%)
  blocking collectives  37.5 us (18%)
  matrix products  20.8 us (10%)
  local copies, waits for them, and re-layouts  13.8 us (7%)
  between operations  13.4 us (6%)
  other arithmetic  10 us (5%)
  starting transfers between devices  3.3 us (2%)
    psum x1, waiting for transfers between devices, per_device(): lax.psum(partial_value.astype(jnp.bfloat16), 'tp').astype(jnp.float32)  33 us
    reduce_scatter x1, waiting for transfers between devices, per_device(): lax.psum_scatter(result.reshape(gathered.shape).astype(jnp.bfloat16), 'tp...  30.7 us
    all_gather x1, waiting for transfers between devices, per_device(): gathered = lax.all_gather(arrived, 'tp', axis=1, tiled=True)  23 us
    all_gather x1, waiting for transfers between devices, per_device(): returned = lax.all_gather(back_rows, 'tp', axis=1, tiled=True)  21.9 us
    all_to_all x1, blocking collectives, per_device(): lax.all_to_all(summed, 'sp', split_axis=0, concat_axis=0, tiled=True)  18.9 us
    all_to_all x1, blocking collectives, per_device(): lax.all_to_all(mine, 'sp', split_axis=0, concat_axis=0, tiled=True)  18.6 us
    dot_general x1, matrix products, per_device(): result = jnp.dot(activated, w_down, preferred_element_type=jnp.float32)  10.5 us
    gather x2, local copies, waits for them, and re-layouts, per_device(): jnp.take(slot_table, slot_index, axis=0).reshape(rows_here, TOP, width)  7.81 us
  transfers between devices with their start and end apart: 5, of which 4 were waited for; matrix products, arithmetic and copies ran while one was open for 3% of the time, Pallas kernels for 0%

commit v1 on v0

v1 whole, which is shorter than its diff:
```python
import functools

import jax
import jax.numpy as jnp
import numpy as np
from jax import lax
from jax.experimental import pallas as pl
from jax.experimental.pallas import tpu as pltpu
from jax.sharding import PartitionSpec as P

HEAD_DIM = 64
WINDOW = 128
TOP = 2
CORES = 2
F32 = jnp.float32
BF16 = jnp.bfloat16
MESH = pl.DeviceIdType.MESH


def kernel(
    S,
    T,
    slope_ref,
    sink_ref,
    q_ref,
    k_ref,
    v_ref,
    res_ref,
    gain_ref,
    routes_ref,
    rw_ref,
    wo_hbm,
    wg_hbm,
    wu_hbm,
    wd_hbm,
    out_ref,
    wo,
    wg,
    wu,
    wd,
    halo,
    att,
    pp,
    rc1,
    sb1,
    ry1,
    mixed,
    picked,
    x_all,
    xn,
    act,
    yp,
    rc2,
    sb2,
    ry2,
    rb,
    ret,
    o_all,
    w_sem,
    halo_s,
    halo_r,
    c1_s,
    c1_r,
    y1_s,
    y1_r,
    a_s,
    a_r,
    fy_s,
    fy_r,
    fc_s,
    fc_r,
    c2_s,
    c2_r,
    y2_s,
    y2_r,
    b_s,
    b_r,
    gy_s,
    gy_r,
    gc_s,
    gc_r,
):
    R, D = res_ref.shape
    Y = T // CORES
    W = D // T
    H = q_ref.shape[1] // HEAD_DIM
    KV = k_ref.shape[1] // HEAD_DIM
    G = H // KV
    C = x_all.shape[0] // S
    half = S // 2
    GM = half * C
    FL = wg.shape[1]

    me = lax.axis_index("sp")
    t = lax.axis_index("tp")
    y = t // CORES
    c = t % CORES
    oc = 1 - c

    def tp_of(yy, cc):
        return yy * CORES + cc

    def cols(tt):
        return pl.ds(pl.multiple_of(tt * W, W), W)

    def rows(s):
        return pl.ds(pl.multiple_of(s * C, C), C)

    def yo(d):
        return (y + d) % Y

    def remote(src, dst, ss, rs, **dev):
        return pltpu.make_async_remote_copy(
            src_ref=src, dst_ref=dst, send_sem=ss, recv_sem=rs, device_id=dev, device_id_type=MESH
        )

    loads = [
        pltpu.make_async_copy(wo_hbm, wo, w_sem.at[0]),
        pltpu.make_async_copy(wg_hbm.at[0], wg, w_sem.at[1]),
        pltpu.make_async_copy(wu_hbm.at[0], wu, w_sem.at[2]),
        pltpu.make_async_copy(wd_hbm.at[0], wd, w_sem.at[3]),
    ]
    for load in loads:
        load.start()

    barrier = pltpu.get_barrier_semaphore()

    @pl.loop(1, S)
    def _(d):
        pl.semaphore_signal(
            barrier, inc=1, device_id={"sp": (me + d) % S}, device_id_type=MESH
        )

    for d in range(1, Y):
        pl.semaphore_signal(
            barrier, inc=1, device_id={"tp": tp_of(yo(d), c)}, device_id_type=MESH
        )
    pl.semaphore_signal(barrier, inc=1, device_id={"tp": tp_of(y, oc)}, device_id_type=MESH)
    pl.semaphore_wait(barrier, S - 1 + Y)

    halo_copies = [
        remote(src, halo.at[i], halo_s.at[i], halo_r.at[i], sp=jnp.minimum(me + 1, S - 1))
        for i, src in enumerate((k_ref, v_ref))
    ]

    @pl.when(me < S - 1)
    def _():
        for copy in halo_copies:
            copy.start()

    r0 = routes_ref[:, 0:1]
    r1 = routes_ref[:, 1:2]
    lane_e = lax.broadcasted_iota(jnp.int32, (R, 128), 1)
    hit0 = lane_e == r0
    hit1 = lane_e == r1
    member = jnp.where(hit0 | hit1, 1.0, 0.0).astype(BF16)
    tri = jnp.where(
        lax.broadcasted_iota(jnp.int32, (R, R), 1) < lax.broadcasted_iota(jnp.int32, (R, R), 0),
        1.0,
        0.0,
    ).astype(BF16)
    rank = jnp.dot(tri, member, preferred_element_type=F32)
    rank0 = jnp.sum(jnp.where(hit0, rank, 0.0), axis=1, keepdims=True)
    rank1 = jnp.sum(jnp.where(hit1, rank, 0.0), axis=1, keepdims=True)
    slot0 = r0.astype(F32) * C + rank0
    slot1 = r1.astype(F32) * C + rank1
    lane_s = lax.broadcasted_iota(jnp.int32, (R, S * C), 1).astype(F32)

    def picker(slot):
        return jnp.where(lane_s == slot, 1.0, 0.0)

    qi = lax.broadcasted_iota(jnp.int32, (R, R), 0)
    kj = lax.broadcasted_iota(jnp.int32, (R, R), 1)
    dist_own = (qi - kj).astype(F32)
    dist_old = (qi - kj + WINDOW).astype(F32)
    nt = (((1,), (1,)), ((), ()))

    @pl.when(me > 0)
    def _():
        for copy in halo_copies:
            copy.wait_recv()

    @pl.when(me == 0)
    def _():
        halo[...] = jnp.zeros_like(halo)

    ok_own = qi >= kj
    ok_old = (kj >= qi) & (kj + me * R >= WINDOW)
    for h in range(H):
        kc = slice((h // G) * HEAD_DIM, (h // G + 1) * HEAD_DIM)
        q = q_ref[:, h * HEAD_DIM : (h + 1) * HEAD_DIM]
        slope = slope_ref[t * H + h]
        s_own = lax.dot_general(q, k_ref[:, kc], nt, preferred_element_type=F32)
        s_old = lax.dot_general(q, halo[0, :, kc], nt, preferred_element_type=F32)
        s_own = jnp.where(ok_own, s_own * HEAD_DIM**-0.5 - slope * dist_own, -jnp.inf)
        s_old = jnp.where(ok_old, s_old * HEAD_DIM**-0.5 - slope * dist_old, -jnp.inf)
        peak = jnp.maximum(
            jnp.max(s_own, axis=1, keepdims=True), jnp.max(s_old, axis=1, keepdims=True)
        )
        e_own = jnp.exp(s_own - peak)
        e_old = jnp.exp(s_old - peak)
        total = jnp.sum(e_own, axis=1, keepdims=True) + jnp.sum(e_old, axis=1, keepdims=True)
        inv = 1.0 / total
        mix = jnp.dot((e_own * inv).astype(BF16), v_ref[:, kc], preferred_element_type=F32)
        mix += jnp.dot((e_old * inv).astype(BF16), halo[1, :, kc], preferred_element_type=F32)
        keep = 1.0 / (1.0 + jnp.exp(sink_ref[h] - peak - jnp.log(total)))
        att[:, h * HEAD_DIM : (h + 1) * HEAD_DIM] = (mix * keep).astype(BF16)

    loads[0].wait()

    def project(tt):
        pp[:, cols(tt)] = jnp.dot(att[...], wo[:, cols(tt)], preferred_element_type=F32).astype(
            BF16
        )

    def c1(yy):
        return remote(
            pp.at[:, cols(tp_of(yy, oc))], rc1.at[yy], c1_s.at[yy], c1_r.at[yy], tp=tp_of(y, oc)
        )

    def y1_send(yy):
        return remote(sb1.at[yy], ry1.at[y], y1_s.at[yy], y1_r.at[y], tp=tp_of(yy, c))

    def y1_recv(yy):
        return remote(sb1.at[yy], ry1.at[yy], y1_s.at[yy], y1_r.at[yy], tp=tp_of(yy, c))

    for d in list(range(1, Y)) + [0]:
        project(tp_of(yo(d), oc))
        c1(yo(d)).start()
    for d in list(range(1, Y)) + [0]:
        project(tp_of(yo(d), c))
    for d in range(1, Y):
        c1(yo(d)).wait_recv()
        sb1[yo(d)] = (pp[:, cols(tp_of(yo(d), c))].astype(F32) + rc1[yo(d)].astype(F32)).astype(
            BF16
        )
        y1_send(yo(d)).start()
    c1(y).wait_recv()
    head_sum = pp[:, cols(t)].astype(F32) + rc1[y].astype(F32)
    for d in range(1, Y):
        y1_recv(yo(d)).wait_recv()
        head_sum = head_sum + ry1[yo(d)].astype(F32)
    mixed[...] = (res_ref[:, cols(t)].astype(F32) + head_sum).astype(BF16)

    both = (picker(slot0) + picker(slot1)).T.astype(BF16)
    picked[...] = jnp.dot(both, mixed[...], preferred_element_type=F32).astype(BF16)

    loc = me % half
    near = (me // half) * half
    far = half - near

    def place(base, d):
        return base + (loc + half - d) % half

    def a_send(e):
        return remote(
            picked.at[rows(e)], x_all.at[rows(me), cols(t)], a_s.at[e], a_r.at[me], sp=e
        )

    def a_recv(s):
        return remote(picked.at[rows(s)], x_all.at[rows(s), cols(t)], a_s.at[s], a_r.at[s], sp=s)

    def fy_send(s, yy):
        ref = x_all.at[rows(s), cols(t)]
        return remote(ref, ref, fy_s.at[s, yy], fy_r.at[s, y], tp=tp_of(yy, c))

    def fy_recv(s, yy):
        ref = x_all.at[rows(s), cols(tp_of(yy, c))]
        return remote(ref, ref, fy_s.at[s, yy], fy_r.at[s, yy], tp=tp_of(yy, c))

    def fc_send(s, yy):
        ref = x_all.at[rows(s), cols(tp_of(yy, c))]
        return remote(ref, ref, fc_s.at[s, yy], fc_r.at[s, yy], tp=tp_of(y, oc))

    def fc_recv(s, yy):
        ref = x_all.at[rows(s), cols(tp_of(yy, oc))]
        return remote(ref, ref, fc_s.at[s, yy], fc_r.at[s, yy], tp=tp_of(y, oc))

    @pl.loop(1, half)
    def _(d):
        a_send(near + (loc + d) % half).start()

    @pl.loop(0, half)
    def _(d):
        a_send(far + (loc + d) % half).start()

    x_all[rows(me), cols(t)] = picked[rows(me)]

    def forward(s):
        for d in range(1, Y):
            fy_send(s, yo(d)).start()
        fc_send(s, y).start()

    def forward_group(base, first):
        @pl.loop(first, half)
        def _(d):
            s = place(base, d)
            a_recv(s).wait_recv()
            forward(s)

    def relay_group(base):
        @pl.loop(0, half)
        def _(d):
            s = place(base, d)
            for i in range(1, Y):
                fy_recv(s, yo(i)).wait_recv()
                fc_send(s, yo(i)).start()

    def norm_group(base):
        @pl.loop(0, half)
        def _(d):
            s = place(base, d)
            for i in range(Y):
                fc_recv(s, yo(i)).wait_recv()
            x = x_all[rows(s)].astype(F32)
            scale = lax.rsqrt(jnp.mean(x * x, axis=1, keepdims=True) + 1e-06)
            xn[rows(s)] = (x * scale * gain_ref[...]).astype(BF16)

    TN = min(256, FL)

    def hidden_group(base):
        at = pl.ds(pl.multiple_of(base * C, C), GM)

        @pl.loop(0, FL // TN)
        def _(n):
            nn = pl.ds(pl.multiple_of(n * TN, TN), TN)
            gate = jnp.dot(xn[at], wg[:, nn], preferred_element_type=F32)
            up = jnp.dot(xn[at], wu[:, nn], preferred_element_type=F32)
            act[:, nn] = (gate / (1.0 + jnp.exp(-gate)) * up).astype(BF16)

    def c2(g, yy):
        return remote(
            yp.at[g, :, cols(tp_of(yy, oc))],
            rc2.at[g, yy],
            c2_s.at[g, yy],
            c2_r.at[g, yy],
            tp=tp_of(y, oc),
        )

    def down_block(g, tt):
        yp[g, :, cols(tt)] = jnp.dot(act[...], wd[:, cols(tt)], preferred_element_type=F32).astype(
            BF16
        )

    def down_group(g):
        @pl.loop(0, Y)
        def _(d):
            yy = yo(d + 1)
            down_block(g, tp_of(yy, oc))
            c2(g, yy).start()

        @pl.loop(0, Y)
        def _(d):
            down_block(g, tp_of(yo(d + 1), c))

    def y2_send(g, p, yy):
        return remote(
            sb2.at[g, yy, rows(p)],
            ry2.at[g, y, rows(p)],
            y2_s.at[g, p, yy],
            y2_r.at[g, p, y],
            tp=tp_of(yy, c),
        )

    def y2_recv(g, p, yy):
        return remote(
            sb2.at[g, yy, rows(p)],
            ry2.at[g, yy, rows(p)],
            y2_s.at[g, p, yy],
            y2_r.at[g, p, yy],
            tp=tp_of(yy, c),
        )

    def b_send(s):
        return remote(rb.at[rows(s)], ret.at[rows(me)], b_s.at[s], b_r.at[me], sp=s)

    def b_recv(s):
        return remote(rb.at[rows(s)], ret.at[rows(s)], b_s.at[s], b_r.at[s], sp=s)

    def pair_sum(g):
        for d in list(range(1, Y)) + [0]:
            yy = yo(d)
            c2(g, yy).wait_recv()

            @pl.loop(0, half)
            def _(i):
                p = (loc + half - i) % half
                sb2[g, yy, rows(p)] = (
                    yp[g, rows(p), cols(tp_of(yy, c))].astype(F32) + rc2[g, yy, rows(p)].astype(F32)
                ).astype(BF16)
                if d:
                    y2_send(g, p, yy).start()

    def send_back(g, base):
        @pl.loop(0, half)
        def _(i):
            p = (loc + half - i) % half
            s = base + p
            total = sb2[g, y, rows(p)].astype(F32)
            for d in range(1, Y):
                y2_recv(g, p, yo(d)).wait_recv()
                total = total + ry2[g, yo(d), rows(p)].astype(F32)
            rb[rows(s)] = total.astype(BF16)

            @pl.when(s != me)
            def _():
                b_send(s).start()

    forward(me)
    forward_group(near, 1)
    relay_group(near)
    norm_group(near)
    loads[1].wait()
    loads[2].wait()
    hidden_group(near)
    loads[3].wait()
    down_group(0)
    forward_group(far, 0)
    pair_sum(0)
    relay_group(far)
    norm_group(far)
    hidden_group(far)
    send_back(0, near)
    down_group(1)
    pair_sum(1)
    send_back(1, far)

    ret[rows(me)] = rb[rows(me)]

    @pl.loop(1, S)
    def _(d):
        b_recv((me + d) % S).wait_recv()

    mix0 = jnp.dot(picker(slot0).astype(BF16), ret[...], preferred_element_type=F32)
    mix1 = jnp.dot(picker(slot1).astype(BF16), ret[...], preferred_element_type=F32)
    o_all[:, cols(t)] = (
        mixed[...].astype(F32) + (rw_ref[:, 0:1] * mix0 + rw_ref[:, 1:2] * mix1)
    ).astype(BF16)

    def gy_send(yy):
        ref = o_all.at[:, cols(t)]
        return remote(ref, ref, gy_s.at[yy], gy_r.at[y], tp=tp_of(yy, c))

    def gy_recv(yy):
        ref = o_all.at[:, cols(tp_of(yy, c))]
        return remote(ref, ref, gy_s.at[yy], gy_r.at[yy], tp=tp_of(yy, c))

    def gc_send(yy):
        ref = o_all.at[:, cols(tp_of(yy, c))]
        return remote(ref, ref, gc_s.at[yy], gc_r.at[yy], tp=tp_of(y, oc))

    def gc_recv(yy):
        ref = o_all.at[:, cols(tp_of(yy, oc))]
        return remote(ref, ref, gc_s.at[yy], gc_r.at[yy], tp=tp_of(y, oc))

    for d in range(1, Y):
        gy_send(yo(d)).start()
    gc_send(y).start()
    for d in range(1, Y):
        gy_recv(yo(d)).wait_recv()
        gc_send(yo(d)).start()
    for d in range(Y):
        gc_recv(yo(d)).wait_recv()
    out_ref[...] = o_all[...]

    @pl.when(me < S - 1)
    def _():
        for copy in halo_copies:
            copy.wait_send()

    for d in range(Y):
        c1(yo(d)).wait_send()
        gc_send(yo(d)).wait_send()
        for g in range(2):
            c2(g, yo(d)).wait_send()
    for d in range(1, Y):
        y1_send(yo(d)).wait_send()
        gy_send(yo(d)).wait_send()

    @pl.loop(1, S)
    def _(d):
        a_send((me + d) % S).wait_send()
        b_send((me + d) % S).wait_send()

    @pl.loop(0, S)
    def _(s):
        for d in range(Y):
            fc_send(s, yo(d)).wait_send()
        for d in range(1, Y):
            fy_send(s, yo(d)).wait_send()

    @pl.loop(0, half)
    def _(p):
        for d in range(1, Y):
            for g in range(2):
                y2_send(g, p, yo(d)).wait_send()


def per_device(
    S,
    T,
    queries,
    key_rows,
    value_rows,
    sink_logits,
    out_weight,
    residual,
    norm_gain,
    routes,
    route_weights,
    gate_weight,
    up_weight,
    down_weight,
):
    R, D = residual.shape
    HW = queries.shape[1]
    heads = HW // HEAD_DIM * T
    Y = T // CORES
    W = D // T
    C = 2 * R * TOP // S
    half = S // 2
    GM = half * C
    FL = gate_weight.shape[2]
    slopes = jnp.asarray(np.exp2(-8.0 * np.arange(1, heads + 1) / heads).astype(np.float32))
    vmem = pl.BlockSpec(memory_space=pltpu.VMEM)
    smem = pl.BlockSpec(memory_space=pltpu.SMEM)
    hbm = pl.BlockSpec(memory_space=pl.ANY)
    dma = pltpu.SemaphoreType.DMA
    v = pltpu.VMEM
    return pl.pallas_call(
        functools.partial(kernel, S, T),
        out_shape=jax.ShapeDtypeStruct((R, D), BF16),
        in_specs=[smem, smem] + [vmem] * 7 + [hbm] * 4,
        out_specs=vmem,
        scratch_shapes=[
            v(out_weight.shape, BF16),
            v(gate_weight.shape[1:], BF16),
            v(up_weight.shape[1:], BF16),
            v(down_weight.shape[1:], BF16),
            v((2,) + key_rows.shape, BF16),
            v((R, HW), BF16),
            v((R, D), BF16),
            v((Y, R, W), BF16),
            v((Y, R, W), BF16),
            v((Y, R, W), BF16),
            v((R, W), BF16),
            v((S * C, W), BF16),
            v((S * C, D), BF16),
            v((S * C, D), BF16),
            v((GM, FL), BF16),
            v((2, GM, D), BF16),
            v((2, Y, GM, W), BF16),
            v((2, Y, GM, W), BF16),
            v((2, Y, GM, W), BF16),
            v((S * C, W), BF16),
            v((S * C, W), BF16),
            v((R, D), BF16),
            dma((4,)),
            dma((2,)),
            dma((2,)),
            dma((Y,)),
            dma((Y,)),
            dma((Y,)),
            dma((Y,)),
            dma((S,)),
            dma((S,)),
            dma((S, Y)),
            dma((S, Y)),
            dma((S, Y)),
            dma((S, Y)),
            dma((2, Y)),
            dma((2, Y)),
            dma((2, half, Y)),
            dma((2, half, Y)),
            dma((S,)),
            dma((S,)),
            dma((Y,)),
            dma((Y,)),
            dma((Y,)),
            dma((Y,)),
        ],
        compiler_params=pltpu.CompilerParams(
            collective_id=0, has_side_effects=True, vmem_limit_bytes=60 * 1024 * 1024
        ),
        name="layer",
    )(
        slopes,
        sink_logits,
        queries,
        key_rows,
        value_rows,
        residual,
        norm_gain.reshape(1, D),
        routes,
        route_weights,
        out_weight,
        gate_weight,
        up_weight,
        down_weight,
    )


def solution(mesh):
    placed = (
        P("sp", "tp"),
        P("sp", "tp"),
        P("sp", "tp"),
        P("tp"),
        P("tp", None),
        P("sp", None),
        P(),
        P("sp", None),
        P("sp", None),
        P("sp", None, "tp"),
        P("sp", None, "tp"),
        P("sp", "tp", None),
    )
    return jax.shard_map(
        functools.partial(per_device, mesh.shape["sp"], mesh.shape["tp"]),
        mesh=mesh,
        in_specs=placed,
        out_specs=P("sp", None),
        check_vma=False,
    )
```

time: 209 us -> 80.7 us (0.39)
  waiting for transfers between devices: 109 us -> 0 us
  Pallas kernels: 0 us -> 75.5 us
  blocking collectives: 37.5 us -> 0 us
  matrix products: 20.8 us -> 0 us
  between operations: 13.4 us -> 0.01 us
  other arithmetic: 10 us -> 0 us
  local copies, waits for them, and re-layouts: 13.8 us -> 4.7 us
  starting transfers between devices: 3.3 us -> 0 us
    pallas_call x0 -> x1, Pallas kernels: none -> 75.5 us  [per_device(): pl.pallas_call(functools.partial(kernel, S, T), out_shape=jax.ShapeDtypeS...]
    all_gather x2 -> x0, waiting for transfers between devices: 44.9 us -> none  [the longest x1 23 us: per_device(): gathered = lax.all_gather(arrived, 'tp', axis=1, tiled=True)]
    all_to_all x2 -> x0, blocking collectives: 37.5 us -> none  [the longest x1 18.9 us: per_device(): lax.all_to_all(summed, 'sp', split_axis=0, concat_axis=0, tiled=True)]
    psum x1 -> x0, waiting for transfers between devices: 33 us -> none  [per_device(): lax.psum(partial_value.astype(jnp.bfloat16), 'tp').astype(jnp.float32)]
    reduce_scatter x1 -> x0, waiting for transfers between devices: 30.7 us -> none  [per_device(): lax.psum_scatter(result.reshape(gathered.shape).astype(jnp.bfloat16), 'tp...]
    dot_general x6 -> x0, matrix products: 20.8 us -> none  [the longest x1 10.5 us: per_device(): result = jnp.dot(activated, w_down, preferred_element_type=jnp.float32)]
    gather x2 -> x0, local copies, waits for them, and re-layouts: 7.81 us -> none  [per_device(): jnp.take(slot_table, slot_index, axis=0).reshape(rows_here, TOP, width)]
    reduce_sum x5 -> x0, other arithmetic: 7.08 us -> none  [the longest x1 5.47 us: per_device(): jnp.sum(route_weights[..., None] * picked.astype(jnp.float32), axis=1)]
  transfers between devices with their start and end apart: 5 -> 0, of which waited for: 4 -> 0; matrix products, arithmetic and copies ran while one was open for 3% -> 0% of each run, Pallas kernels for 0% -> 0%
where the time goes in v1:
time: 80.7 us; the launch traced here: 80.2 us
  Pallas kernels  75.5 us (94%)
  local copies, waits for them, and re-layouts  4.7 us (6%)
    pallas_call x1, Pallas kernels, per_device(): pl.pallas_call(functools.partial(kernel, S, T), out_shape=jax.ShapeDtypeS...  75.5 us
    unnamed x3, local copies, waits for them, and re-layouts  4.7 us

profile of v1, /device:TPU:3, one launch (start us, length us, event | category | flops | bytes accessed | tf_op | source)
XLA Modules:
  0.0 80.2 jit_solution(7033358322640939042)
XLA Ops:
  0.0 1.4 %copy.14.routes_ref = s32[128,2]{1,0:T(8,128)} copy(s32[128,2]{0,1:T(2,128)} %param.20) | data formatting | bytes 2048 | tf_op args[7]
  1.4 1.4 %copy.15.rw_ref = f32[128,2]{1,0:T(8,128)} copy(f32[128,2]{0,1:T(2,128)} %param.21) | data formatting | bytes 2048 | tf_op args[8]
  2.8 75.5 %layer.1 = bf16[128,2048]{1,0:T(8,128)(2,1)} custom-call(f32[32]{0:T(128)} %constant.2.clone.slope_ref, f32[8]{0:T(128)} %sink_ref.1, bf16[128,512]{1,0:T(8,128)(2,1)} %q_ref.1, bf16[128,256]{1,0:T(8,128)(2,1)} %k_ref.1, bf16[128,256]{1,0:T(8,128)(2,1)} %v_ref.1, bf16[128,2048]{1,0:T(8,128)(2,1)} %res_ref.1, f32[1,2048]{1,0:T(1,128)} %bitcast.1, ...), custom_call_target="tpu_custom_call" | custom-call | tf_op jit(solution)/shard_map/layer/pallas_call | solution.py:530
  78.3 1.9 %copy.17 = bf16[128,2048]{1,0:T(8,128)(2,1)} copy(bf16[128,2048]{1,0:T(8,128)(2,1)} %layer.1) | data formatting | bytes 1048576

commit v2 on v1

--- a/solution.py
+++ b/solution.py
@@ -148,8 +148,11 @@
         for copy in halo_copies:
             copy.start()
 
-    r0 = routes_ref[:, 0:1]
-    r1 = routes_ref[:, 1:2]
+    def column(row):
+        return jnp.broadcast_to(row, (R, R)).T[:, 0:1]
+
+    r0 = column(routes_ref[0:1, :].astype(F32)).astype(jnp.int32)
+    r1 = column(routes_ref[1:2, :].astype(F32)).astype(jnp.int32)
     lane_e = lax.broadcasted_iota(jnp.int32, (R, 128), 1)
     hit0 = lane_e == r0
     hit1 = lane_e == r1
@@ -175,6 +178,21 @@
     dist_old = (qi - kj + WINDOW).astype(F32)
     nt = (((1,), (1,)), ((), ()))
 
+    ok_own = qi >= kj
+    ok_old = (kj >= qi) & (kj + me * R >= WINDOW)
+
+    def head(h):
+        return slice(h * HEAD_DIM, (h + 1) * HEAD_DIM), slice(
+            (h // G) * HEAD_DIM, (h // G + 1) * HEAD_DIM
+        )
+
+    def scores(h, keys, dist, ok):
+        raw = lax.dot_general(q_ref[:, head(h)[0]], keys, nt, preferred_element_type=F32)
+        return jnp.where(ok, raw * HEAD_DIM**-0.5 - slope_ref[t * H + h] * dist, -jnp.inf)
+
+    own = [scores(h, k_ref[:, head(h)[1]], dist_own, ok_own) for h in range(H)]
+    own_peak = [jnp.max(x, axis=1, keepdims=True) for x in own]
+
     @pl.when(me > 0)
     def _():
         for copy in halo_copies:
@@ -184,19 +202,11 @@
     def _():
         halo[...] = jnp.zeros_like(halo)
 
-    ok_own = qi >= kj
-    ok_old = (kj >= qi) & (kj + me * R >= WINDOW)
     for h in range(H):
-        kc = slice((h // G) * HEAD_DIM, (h // G + 1) * HEAD_DIM)
-        q = q_ref[:, h * HEAD_DIM : (h + 1) * HEAD_DIM]
-        slope = slope_ref[t * H + h]
-        s_own = lax.dot_general(q, k_ref[:, kc], nt, preferred_element_type=F32)
-        s_old = lax.dot_general(q, halo[0, :, kc], nt, preferred_element_type=F32)
-        s_own = jnp.where(ok_own, s_own * HEAD_DIM**-0.5 - slope * dist_own, -jnp.inf)
-        s_old = jnp.where(ok_old, s_old * HEAD_DIM**-0.5 - slope * dist_old, -jnp.inf)
-        peak = jnp.maximum(
-            jnp.max(s_own, axis=1, keepdims=True), jnp.max(s_old, axis=1, keepdims=True)
-        )
+        hc, kc = head(h)
+        s_own = own[h]
+        s_old = scores(h, halo[0, :, kc], dist_old, ok_old)
+        peak = jnp.maximum(own_peak[h], jnp.max(s_old, axis=1, keepdims=True))
         e_own = jnp.exp(s_own - peak)
         e_old = jnp.exp(s_old - peak)
         total = jnp.sum(e_own, axis=1, keepdims=True) + jnp.sum(e_old, axis=1, keepdims=True)
@@ -204,7 +214,7 @@
         mix = jnp.dot((e_own * inv).astype(BF16), v_ref[:, kc], preferred_element_type=F32)
         mix += jnp.dot((e_old * inv).astype(BF16), halo[1, :, kc], preferred_element_type=F32)
         keep = 1.0 / (1.0 + jnp.exp(sink_ref[h] - peak - jnp.log(total)))
-        att[:, h * HEAD_DIM : (h + 1) * HEAD_DIM] = (mix * keep).astype(BF16)
+        att[:, hc] = (mix * keep).astype(BF16)
 
     loads[0].wait()
 
@@ -245,66 +255,66 @@
     both = (picker(slot0) + picker(slot1)).T.astype(BF16)
     picked[...] = jnp.dot(both, mixed[...], preferred_element_type=F32).astype(BF16)
 
-    loc = me % half
-    near = (me // half) * half
-    far = half - near
-
-    def place(base, d):
-        return base + (loc + half - d) % half
+    loc = me // 2
+    near = me % 2
+    far = 1 - near
+
+    def source(par, p):
+        return 2 * p + par
+
+    def place(par, d):
+        return source(par, (loc + half - d) % half)
+
+    def spot(s):
+        return rows((s % 2) * half + s // 2)
 
     def a_send(e):
         return remote(
-            picked.at[rows(e)], x_all.at[rows(me), cols(t)], a_s.at[e], a_r.at[me], sp=e
+            picked.at[rows(e)], x_all.at[spot(me), cols(t)], a_s.at[e], a_r.at[me], sp=e
         )
 
     def a_recv(s):
-        return remote(picked.at[rows(s)], x_all.at[rows(s), cols(t)], a_s.at[s], a_r.at[s], sp=s)
+        return remote(picked.at[rows(s)], x_all.at[spot(s), cols(t)], a_s.at[s], a_r.at[s], sp=s)
 
     def fy_send(s, yy):
-        ref = x_all.at[rows(s), cols(t)]
+        ref = x_all.at[spot(s), cols(t)]
         return remote(ref, ref, fy_s.at[s, yy], fy_r.at[s, y], tp=tp_of(yy, c))
 
     def fy_recv(s, yy):
-        ref = x_all.at[rows(s), cols(tp_of(yy, c))]
+        ref = x_all.at[spot(s), cols(tp_of(yy, c))]
         return remote(ref, ref, fy_s.at[s, yy], fy_r.at[s, yy], tp=tp_of(yy, c))
 
     def fc_send(s, yy):
-        ref = x_all.at[rows(s), cols(tp_of(yy, c))]
+        ref = x_all.at[spot(s), cols(tp_of(yy, c))]
         return remote(ref, ref, fc_s.at[s, yy], fc_r.at[s, yy], tp=tp_of(y, oc))
 
     def fc_recv(s, yy):
-        ref = x_all.at[rows(s), cols(tp_of(yy, oc))]
+        ref = x_all.at[spot(s), cols(tp_of(yy, oc))]
         return remote(ref, ref, fc_s.at[s, yy], fc_r.at[s, yy], tp=tp_of(y, oc))
 
     @pl.loop(1, half)
     def _(d):
-        a_send(near + (loc + d) % half).start()
+        a_send(source(near, (loc + d) % half)).start()
 
     @pl.loop(0, half)
     def _(d):
-        a_send(far + (loc + d) % half).start()
-
-    x_all[rows(me), cols(t)] = picked[rows(me)]
+        a_send(source(far, (loc + d) % half)).start()
+
+    x_all[spot(me), cols(t)] = picked[rows(me)]
 
     def forward(s):
         for d in range(1, Y):
             fy_send(s, yo(d)).start()
         fc_send(s, y).start()
 
-    def forward_group(base, first):
-        @pl.loop(first, half)
-        def _(d):
-            s = place(base, d)
-            a_recv(s).wait_recv()
-            forward(s)
-
-    def relay_group(base):
-        @pl.loop(0, half)
-        def _(d):
-            s = place(base, d)
-            for i in range(1, Y):
-                fy_recv(s, yo(i)).wait_recv()
-                fc_send(s, yo(i)).start()
+    def relay(s):
+        for i in range(1, Y):
+            fy_recv(s, yo(i)).wait_recv()
+            fc_send(s, yo(i)).start()
+
+    def arrive(s):
+        a_recv(s).wait_recv()
+        forward(s)
 
     def norm_group(base):
         @pl.loop(0, half)
@@ -312,14 +322,14 @@
             s = place(base, d)
             for i in range(Y):
                 fc_recv(s, yo(i)).wait_recv()
-            x = x_all[rows(s)].astype(F32)
+            x = x_all[spot(s)].astype(F32)
             scale = lax.rsqrt(jnp.mean(x * x, axis=1, keepdims=True) + 1e-06)
-            xn[rows(s)] = (x * scale * gain_ref[...]).astype(BF16)
+            xn[spot(s)] = (x * scale * gain_ref[...]).astype(BF16)
 
     TN = min(256, FL)
 
     def hidden_group(base):
-        at = pl.ds(pl.multiple_of(base * C, C), GM)
+        at = pl.ds(pl.multiple_of(base * GM, GM), GM)
 
         @pl.loop(0, FL // TN)
         def _(n):
@@ -395,7 +405,7 @@
         @pl.loop(0, half)
         def _(i):
             p = (loc + half - i) % half
-            s = base + p
+            s = source(base, p)
             total = sb2[g, y, rows(p)].astype(F32)
             for d in range(1, Y):
                 y2_recv(g, p, yo(d)).wait_recv()
@@ -407,18 +417,29 @@
                 b_send(s).start()
 
     forward(me)
-    forward_group(near, 1)
-    relay_group(near)
+
+    @pl.loop(1, half)
+    def _(d):
+        arrive(place(near, d))
+
+    @pl.loop(0, half)
+    def _(d):
+        relay(place(near, d))
+        arrive(place(far, d))
+
     norm_group(near)
     loads[1].wait()
     loads[2].wait()
     hidden_group(near)
+
+    @pl.loop(0, half)
+    def _(d):
+        relay(place(far, d))
+
     loads[3].wait()
     down_group(0)
-    forward_group(far, 0)
+    norm_group(far)
     pair_sum(0)
-    relay_group(far)
-    norm_group(far)
     hidden_group(far)
     send_back(0, near)
     down_group(1)
@@ -434,7 +455,7 @@
     mix0 = jnp.dot(picker(slot0).astype(BF16), ret[...], preferred_element_type=F32)
     mix1 = jnp.dot(picker(slot1).astype(BF16), ret[...], preferred_element_type=F32)
     o_all[:, cols(t)] = (
-        mixed[...].astype(F32) + (rw_ref[:, 0:1] * mix0 + rw_ref[:, 1:2] * mix1)
+        mixed[...].astype(F32) + (column(rw_ref[0:1, :]) * mix0 + column(rw_ref[1:2, :]) * mix1)
     ).astype(BF16)
 
     def gy_send(yy):
@@ -591,8 +612,8 @@
         value_rows,
         residual,
         norm_gain.reshape(1, D),
-        routes,
-        route_weights,
+        routes.T,
+        route_weights.T,
         out_weight,
         gate_weight,
         up_weight,

time: 80.7 us -> 71.9 us (0.89)
  Pallas kernels: 75.5 us -> 69.8 us
  local copies, waits for them, and re-layouts: 4.7 us -> 1.88 us
    pallas_call x1, Pallas kernels: 75.5 us -> 69.8 us  [per_device(): pl.pallas_call(functools.partial(kernel, S, T), out_shape=jax.ShapeDtypeS...]
    unnamed x3 -> x1, local copies, waits for them, and re-layouts: 4.7 us -> 1.88 us
where the time goes in v2:
time: 71.9 us; the launch traced here: 71.7 us
  Pallas kernels  69.8 us (97%)
  local copies, waits for them, and re-layouts  1.88 us (3%)
    pallas_call x1, Pallas kernels, per_device(): pl.pallas_call(functools.partial(kernel, S, T), out_shape=jax.ShapeDtypeS...  69.8 us
    unnamed x1, local copies, waits for them, and re-layouts  1.88 us

profile of v2, /device:TPU:3, one launch (start us, length us, event | category | flops | bytes accessed | tf_op | source)
XLA Modules:
  0.0 71.7 jit_solution(6503967542551270175)
XLA Ops:
  0.0 69.8 %layer.1 = bf16[128,2048]{1,0:T(8,128)(2,1)} custom-call(f32[32]{0:T(128)} %constant.2.clone.slope_ref, f32[8]{0:T(128)} %sink_ref.1, bf16[128,512]{1,0:T(8,128)(2,1)} %q_ref.1, bf16[128,256]{1,0:T(8,128)(2,1)} %k_ref.1, bf16[128,256]{1,0:T(8,128)(2,1)} %v_ref.1, bf16[128,2048]{1,0:T(8,128)(2,1)} %res_ref.1, f32[1,2048]{1,0:T(1,128)} %bitcast.3, ...), custom_call_target="tpu_custom_call" | custom-call | tf_op jit(solution)/shard_map/layer/pallas_call | solution.py:551
  69.9 1.9 %copy.15 = bf16[128,2048]{1,0:T(8,128)(2,1)} copy(bf16[128,2048]{1,0:T(8,128)(2,1)} %layer.1) | data formatting | bytes 1048576

commit v3 on v2

--- a/solution.py
+++ b/solution.py
@@ -432,14 +432,15 @@
     loads[2].wait()
     hidden_group(near)
 
-    @pl.loop(0, half)
-    def _(d):
-        relay(place(far, d))
-
     loads[3].wait()
     down_group(0)
+
+    @pl.loop(0, half)
+    def _(d):
+        relay(place(far, d))
+
+    pair_sum(0)
     norm_group(far)
-    pair_sum(0)
     hidden_group(far)
     send_back(0, near)
     down_group(1)

time: 71.9 us -> 71.2 us (level)
  no operation moved by 1% of the time
where the time goes in v3:
time: 71.2 us; the launch traced here: 71 us
  Pallas kernels  69.1 us (97%)
  local copies, waits for them, and re-layouts  1.88 us (3%)
    pallas_call x1, Pallas kernels, per_device(): pl.pallas_call(functools.partial(kernel, S, T), out_shape=jax.ShapeDtypeS...  69.1 us
    unnamed x1, local copies, waits for them, and re-layouts  1.88 us

profile of v3, /device:TPU:3, one launch (start us, length us, event | category | flops | bytes accessed | tf_op | source)
XLA Modules:
  0.0 71.0 jit_solution(13217109295726205745)
XLA Ops:
  0.0 69.1 %layer.1 = bf16[128,2048]{1,0:T(8,128)(2,1)} custom-call(f32[32]{0:T(128)} %constant.2.clone.slope_ref, f32[8]{0:T(128)} %sink_ref.1, bf16[128,512]{1,0:T(8,128)(2,1)} %q_ref.1, bf16[128,256]{1,0:T(8,128)(2,1)} %k_ref.1, bf16[128,256]{1,0:T(8,128)(2,1)} %v_ref.1, bf16[128,2048]{1,0:T(8,128)(2,1)} %res_ref.1, f32[1,2048]{1,0:T(1,128)} %bitcast.3, ...), custom_call_target="tpu_custom_call" | custom-call | tf_op jit(solution)/shard_map/layer/pallas_call | solution.py:552
  69.1 1.9 %copy.15 = bf16[128,2048]{1,0:T(8,128)(2,1)} copy(bf16[128,2048]{1,0:T(8,128)(2,1)} %layer.1) | data formatting | bytes 1048576
